TPU v7x, 512 devices: a whole 4x4x16 slice. The times are simulated.
512 devices in a mesh: ep: 32 (over z, core), tp: 16 (over y, x).
Axes of the slice: x: 4, y: 4, z: 16, core: 2. Of those that a mesh axis runs over, the one named last changes fastest.
Arguments:
- mix_in: bfloat16 [4096, 2048], P('ep'), may hold values from -6 to 6
- mix_gain: float32 [2048], replicated, may hold values from 0.1 to 1.9
- lam_re: float32 [128, 64], P('tp'), may hold values from -0.34 to -1e-05
- lam_im: float32 [128, 64], P('tp'), may hold values from 0.2 to 4
- log_dt: float32 [128], P('tp'), may hold values from -2.31 to 0
- b_re: float32 [128, 64, 16], P('tp'), may hold values from -0.0625 to 0.0625
- b_im: float32 [128, 64, 16], P('tp'), may hold values from -0.0625 to 0.0625
- c_re: float32 [128, 16, 64], P('tp'), may hold values from -0.5 to 0.5
- c_im: float32 [128, 16, 64], P('tp'), may hold values from -0.5 to 0.5
- d_skip: float32 [2048], P('tp'), may hold values from -2 to 2
- log_retain: float32 [4096, 128], P('ep', 'tp'), may hold values from -2.2 to 0
- w_lin: bfloat16 [2048, 2048], P(None, 'tp'), may hold values from -0.125 to 0.125
- w_glu: bfloat16 [2048, 2048], P(None, 'tp'), may hold values from -0.125 to 0.125
- moe_in: bfloat16 [4096, 2048], P('ep'), may hold values from -6 to 6
- moe_gain: float32 [2048], replicated, may hold values from 0.1 to 1.9
- routes: int32 [4096, 2], P('ep'), may hold values from 0 to 31, all different within a row; in each aligned block of 128 rows (0 to 127, 128 to 255, ...) at most 12 rows name the same one
- route_weight: float32 [4096, 2], P('ep'), may hold values from 0.1 to 1
- w_gate: bfloat16 [32, 2048, 4096], P('ep', None, 'tp'), may hold values from -0.125 to 0.125
- w_up: bfloat16 [32, 2048, 4096], P('ep', None, 'tp'), may hold values from -0.125 to 0.125
- w_down: bfloat16 [32, 4096, 2048], P('ep', 'tp'), may hold values from -0.09375 to 0.09375
Outputs:
- mix_out: bfloat16 [4096, 2048], P('ep', 'tp')
- moe_out: bfloat16 [4096, 2048], P('ep', 'tp')
Inputs may be any that keep to these rules, and one draw needn't show every extreme that they name: `routes`: each row names 2 different experts. In each aligned block of 128 rows (the rows of one index of ep) no expert is named by more than 12 rows, and in some block an expert is named by exactly 12 rows.
All inputs are finite; a program needn't handle non-finite values.
Results may differ from a plain program's by a relative error of at most 0.015.
Values may be sent and summed in bfloat16 or wider, within the bound.
A program may use at most 128 MiB of HBM per device.

v0:
```python
import functools

import jax
import jax.numpy as jnp
from jax import lax
from jax.experimental import pallas as pl
from jax.experimental.pallas import tpu as pltpu
from jax.sharding import Mesh
from jax.sharding import PartitionSpec as P

EP = ("z", "c")
TP = ("y", "x")
MESH = pl.DeviceIdType.MESH
PAD = 16
LANES = 128
EPS = 1e-06
HIGHEST = lax.Precision.HIGHEST


def cols(index):
    return pl.ds(pl.multiple_of(index * LANES, LANES), LANES)


def exact_dot(a, b, contract=((1,), (0,))):
    return lax.dot_general(
        a, b, (contract, ((), ())), precision=HIGHEST, preferred_element_type=jnp.float32
    )


def fast_dot(a, b):
    return jnp.dot(a, b, preferred_element_type=jnp.float32)


def ones_where(mask, dtype):
    return jnp.where(mask, 1.0, 0.0).astype(dtype)


def times(a, b):
    return (a[0] * b[0] - a[1] * b[1], a[0] * b[1] + a[1] * b[0])


def iota(shape, axis):
    return lax.broadcasted_iota(jnp.int32, shape, axis)


def exchange_kernel(sizes, count, *refs):
    nz, nc, ny, nx, cap, pieces = sizes
    experts, tp = nz * nc, ny * nx
    slots = experts * cap
    half = slots // 2
    batch = experts // pieces
    high, low = batch * cap, batch * cap // 2
    sources, refs = refs[:count], refs[count:]
    (mix_ref, moe_ref), refs = refs[:2], refs[2:]
    staged, refs = refs[: count - 2], refs[count - 2 :]
    (mix_w, blend, powers, partial, fading, message, outgoing, incoming, carries), refs = (
        refs[:9],
        refs[9:],
    )
    (gathered, parts, first_a, first_b, sum_a, sum_b, second_a, second_b), refs = refs[:8], refs[8:]
    (going_back, returned, active, load_sem, z_sent, z_recv, carry_sem, act_sem), refs = (
        refs[:8],
        refs[8:],
    )
    ag_near, ag_far, ag_sent, rs_near, rs_far, rs_sent = refs
    (routes, weights, moe_in, moe_gain, mix_in, mix_gain, retain, lam_re, lam_im), rest = (
        staged[:9],
        staged[9:],
    )
    log_dt, b_re, b_im, c_re, c_im, skip, gate_w, up_w, down_w = rest

    mz, mc = lax.axis_index("z"), lax.axis_index("c")
    my, mx = lax.axis_index("y"), lax.axis_index("x")
    me = mz * nc + mc
    mt = my * nx + mx

    loads = [
        pltpu.make_async_copy(sources[i], staged[i], load_sem.at[i]) for i in range(count - 2)
    ]
    loads += [
        pltpu.make_async_copy(
            sources[count - 2 + i], mix_w.at[:, pl.ds(i * LANES, LANES)], load_sem.at[count - 2 + i]
        )
        for i in range(2)
    ]
    for load in loads:
        load.start()

    def along_z(k):
        peer = lax.rem(me + k, experts)
        return {"z": lax.div(peer, nc), "c": lax.rem(peer, nc)}

    def in_plane(k):
        peer = lax.rem(mt + k, tp)
        return {"y": lax.div(peer, nx), "x": lax.rem(peer, nx)}

    barrier = pltpu.get_barrier_semaphore()
    reach = experts // 2

    @pl.loop(0, reach)
    def _(k):
        pl.semaphore_signal(barrier, inc=1, device_id=along_z(reach + k), device_id_type=MESH)

        @pl.when(k > 0)
        def _():
            pl.semaphore_signal(barrier, inc=1, device_id=along_z(reach - k), device_id_type=MESH)

    @pl.loop(1, tp)
    def _(k):
        pl.semaphore_signal(barrier, inc=1, device_id=in_plane(k), device_id_type=MESH)

    for load in loads[:4]:
        load.wait()
    tokens = moe_in.shape[0]
    expert_row = iota((experts, tokens), 0)
    named = [expert_row == routes[k : k + 1, :] for k in range(2)]
    ahead = iota((tokens, tokens), 0) < iota((tokens, tokens), 1)
    counted = fast_dot(
        ones_where(named[0] | named[1], jnp.bfloat16), ones_where(ahead, jnp.bfloat16)
    )
    targets = [
        routes[k : k + 1, :].astype(jnp.float32) * PAD
        + jnp.sum(jnp.where(named[k], counted, 0.0), axis=0, keepdims=True)
        for k in range(2)
    ]
    sub = iota((LANES, tokens), 0)
    rows = jnp.where(
        sub < 2,
        jnp.where(sub == 0, targets[0], targets[1]),
        jnp.where(sub == 2, weights[0:1, :], weights[1:2, :]),
    )
    down_rows = jnp.transpose(rows)
    wide = iota((tokens, experts * PAD), 1)
    blend[...] = sum(
        jnp.where(wide == down_rows[:, k : k + 1].astype(jnp.int32), down_rows[:, k + 2 : k + 3], 0.0)
        for k in range(2)
    )

    def own_features(source, gain_ref):
        squares = jnp.zeros((source.shape[0], LANES), jnp.float32)
        for f in range(tp):
            piece = source[:, f * LANES : (f + 1) * LANES].astype(jnp.float32)
            squares = squares + piece * piece
        mean = jnp.sum(squares, axis=1, keepdims=True) / source.shape[1]
        own = source[:, cols(mt)].astype(jnp.float32)
        return (own * lax.rsqrt(mean + EPS) * gain_ref[:, cols(mt)]).astype(jnp.bfloat16)

    place = iota((experts * PAD, tokens), 0)
    picked = (place == targets[0].astype(jnp.int32)) | (place == targets[1].astype(jnp.int32))
    chosen = fast_dot(ones_where(picked, jnp.bfloat16), own_features(moe_in, moe_gain))
    outgoing[...] = chosen.astype(jnp.bfloat16).reshape(experts, PAD, LANES)
    incoming[0] = outgoing[me]

    for load in loads[4:15]:
        load.wait()
    inputs = own_features(mix_in, mix_gain).astype(jnp.float32)
    length, groups = inputs.shape[0], lam_re.shape[0]
    each = LANES // groups
    time_step = jnp.exp(jnp.transpose(log_dt[...]))
    log_mag, angle = lam_re[...] * time_step, lam_im[...] * time_step
    half_sine, cosine, sine = jnp.sin(0.5 * angle), jnp.cos(angle), jnp.sin(angle)
    grown, shrunk = jnp.exp(log_mag), jnp.exp(-log_mag)
    minus_re = jnp.tanh(0.5 * log_mag) * (grown + 1.0) * cosine - 2.0 * half_sine * half_sine
    minus_im = grown * sine
    denom = lam_re[...] * lam_re[...] + lam_im[...] * lam_im[...]
    coef_re = (minus_re * lam_re[...] + minus_im * lam_im[...]) / denom
    coef_im = (minus_im * lam_re[...] - minus_re * lam_im[...]) / denom

    def per_channel(values):
        width = values.shape[1]
        return jnp.concatenate(
            [jnp.broadcast_to(values[g : g + 1, :], (each, width)) for g in range(groups)], axis=0
        )

    drive = jnp.concatenate(
        times((per_channel(coef_re), per_channel(coef_im)), (b_re[...], b_im[...])), axis=1
    )
    read = jnp.concatenate([c_re[...], -c_im[...]], axis=1)

    def twice(values):
        return jnp.concatenate([values, values], axis=1)

    grow = [(twice(grown * cosine), twice(grown * sine))]
    shrink = [(twice(shrunk * cosine), twice(-shrunk * sine))]
    for _ in range(7):
        grow.append(times(grow[-1], grow[-1]))
        shrink.append(times(shrink[-1], shrink[-1]))
    sign = jnp.where(iota((1, LANES), 1) < LANES // 2, -1.0, 1.0)
    sixteen = iota((16, LANES), 0)

    def ladder(bases, start, stride, g):
        lower = (jnp.ones((16, LANES), jnp.float32), jnp.zeros((16, LANES), jnp.float32))
        for i in range(4):
            on = (sixteen & (1 << i)) > 0
            row = [part[g : g + 1, :] for part in bases[i]]
            lower = times(lower, (jnp.where(on, row[0], 1.0), jnp.where(on, row[1], 0.0)))
        upper = tuple(part[g : g + 1, :] for part in start)
        step = tuple(part[g : g + 1, :] for part in stride)
        blocks = []
        for _ in range(length // 16):
            blocks.append(times(lower, upper))
            upper = times(upper, step)
        return [jnp.concatenate([b[i] for b in blocks], axis=0) for i in range(2)]

    later, sooner = iota((length, length), 0), iota((length, length), 1)
    causal = later >= sooner
    summed_across = exact_dot(per_channel(retain[...]), ones_where(later <= sooner, jnp.float32))
    summed = jnp.transpose(summed_across)
    fading[...] = jnp.exp(summed)
    group_of = lax.shift_right_logical(iota((LANES, LANES), 0), 4)

    def of_group(values, g):
        return jnp.where(group_of == g, values, 0.0)

    total = skip[...] * inputs
    for g in range(groups):
        at = g * each
        push = exact_dot(inputs, of_group(drive, g))
        down_re, down_im = ladder(shrink, grow[6], shrink[4], g)
        seed = push * down_re + pltpu.roll(push, LANES // 2, 1) * (down_im * sign)
        gap = jnp.minimum(summed[:, at : at + 1] - summed_across[at : at + 1, :], 0.0)
        held = exact_dot(jnp.where(causal, jnp.exp(gap), 0.0), seed)
        up_re, up_im = ladder(grow, shrink[6], grow[4], g)
        up_im = up_im * sign
        powers[0, g] = up_re
        powers[1, g] = up_im
        states = held * up_re + pltpu.roll(held, LANES // 2, 1) * up_im
        total = total + exact_dot(states, of_group(read, g), ((1,), (1,)))
        message[g : g + 1, :] = states[length - 1 : length, :]
        message[groups + g : groups + g + 1, :] = jnp.broadcast_to(
            fading[length - 1 : length, at : at + 1], (1, LANES)
        )
    partial[...] = total
    pl.semaphore_wait(barrier, experts + tp - 2)

    def settle(ref, sem):
        pltpu.make_async_copy(ref, ref, sem).wait()

    def remote(src, dst, sent, landed, peer):
        return pltpu.make_async_remote_copy(
            src_ref=src,
            dst_ref=dst,
            send_sem=sent,
            recv_sem=landed,
            device_id=peer,
            device_id_type=MESH,
        )

    def step_of(j):
        p = lax.div(j, nc)
        return lax.div(p + 1, 2) * (2 * lax.rem(p, 2) - 1)

    def at_slot(j, direction):
        z = lax.rem(mz + direction * step_of(j) + nz, nz)
        return {"z": z, "c": lax.rem(mc + lax.rem(j, nc), nc)}

    for q in range(pieces):

        @pl.loop(q * batch if q else 1, (q + 1) * batch)
        def _(j):
            peer = at_slot(j, -1)
            block = outgoing.at[peer["z"] * nc + peer["c"]]
            remote(block, incoming.at[j], z_sent.at[0], z_recv.at[q], peer).start()

    def carry_to(k):
        return remote(
            message, carries.at[me], carry_sem.at[0, k], carry_sem.at[1, me], along_z(k)
        )

    @pl.loop(1, experts)
    def _(k):
        @pl.when(me + k < experts)
        def _():
            carry_to(k).start()

    def spot(side, q):
        return pl.ds(q * high + side * low, low)

    def inner(q):
        return pl.ds(q * low, low)

    slot_row, slot_column = iota((high, batch * PAD), 0), iota((high, batch * PAD), 1)
    origin = lax.shift_right_logical(slot_row * 5462, 16)
    packing = ones_where(slot_column == origin * PAD + (slot_row - origin * cap), jnp.bfloat16)
    slot_row, slot_column = iota((batch * PAD, high), 0), iota((batch * PAD, high), 1)
    origin = lax.shift_right_logical(slot_row, 4)
    within = slot_row - origin * PAD
    spreading = ones_where((within < cap) & (slot_column == origin * cap + within), jnp.bfloat16)

    def beside(side, k):
        if side == 0:
            return {"x": lax.rem(mx + k, nx)}
        return {"y": lax.rem(my + k, ny)}

    spans = (nx, ny)

    def near_copy(side, q, k):
        block = gathered.at[spot(side, q), cols(mt)]
        return remote(block, block, ag_sent.at[0], ag_near.at[q, side, k], beside(side, k))

    def forward(side, q, source):
        for k in range(1, spans[1 - side]):
            block = gathered.at[spot(side, q), cols(source)]
            remote(block, block, ag_sent.at[0], ag_far.at[q, side], beside(1 - side, k)).start()

    def dispatch_stage(q):
        low_slot = q * batch if q else 1
        settle(incoming.at[pl.ds(low_slot, (q + 1) * batch - low_slot)], z_recv.at[q])
        blocks = incoming[q * batch : (q + 1) * batch].reshape(batch * PAD, LANES)
        packed = fast_dot(packing, blocks).astype(jnp.bfloat16)
        gathered[pl.ds(q * high, high), cols(mt)] = packed
        for side in range(2):
            for k in range(1, spans[side]):
                near_copy(side, q, k).start()
        for side in range(2):
            forward(side, q, mt)

    def forward_stage(q):
        for k in range(1, max(nx, ny)):
            for side in range(2):
                if k < spans[side]:
                    near_copy(side, q, k).wait_recv()
                    if side == 0:
                        source = my * nx + lax.rem(mx - k + nx, nx)
                    else:
                        source = lax.rem(my - k + ny, ny) * nx + mx
                    forward(side, q, source)

    def expert_stage(q):
        for side in range(2):
            distant = spans[side] * (spans[1 - side] - 1) * LANES
            settle(gathered.at[spot(side, q), pl.ds(0, distant)], ag_far.at[q, side])
        if q == 0:
            for load in loads[15:18]:
                load.wait()
        features = gathered[q * high : (q + 1) * high, :]
        gate = fast_dot(features, gate_w[...])
        up = fast_dot(features, up_w[...])
        hidden = (gate * jax.nn.sigmoid(gate) * up).astype(jnp.bfloat16)
        for at in range(tp // 2):
            down = fast_dot(hidden, down_w[:, at * 2 * LANES : (at + 1) * 2 * LANES])
            down = down.astype(jnp.bfloat16)
            for i in range(2):
                f = at * 2 + i
                parts[f // nx, f % nx, q * high : (q + 1) * high, :] = down[
                    :, i * LANES : (i + 1) * LANES
                ]
        for k in range(1, max(nx, ny)):
            for side in range(2):
                if k < spans[side]:
                    peer = beside(side, k)
                    if side == 0:
                        src, dst = parts.at[:, peer["x"], spot(0, q)], first_a.at[k - 1, :, inner(q)]
                    else:
                        src, dst = parts.at[peer["y"], :, spot(1, q)], first_b.at[k - 1, :, inner(q)]
                    remote(src, dst, rs_sent.at[side], rs_near.at[q, side], peer).start()

    def sum_stage(q):
        for side in range(2):
            firsts = (first_a, first_b)[side]
            sums = (sum_a, sum_b)[side]
            seconds = (second_a, second_b)[side]
            settle(firsts.at[:, :, inner(q)], rs_near.at[q, side])
            for j in range(spans[1 - side]):
                own = parts[j, mx, spot(0, q), :] if side == 0 else parts[my, j, spot(1, q), :]
                summed = own.astype(jnp.float32)
                for k in range(spans[side] - 1):
                    summed = summed + firsts[k, j, inner(q), :].astype(jnp.float32)
                sums[j, inner(q), :] = summed.astype(jnp.bfloat16)
            for k in range(1, spans[1 - side]):
                peer = beside(1 - side, k)
                far = peer["y"] if side == 0 else peer["x"]
                remote(
                    sums.at[far, inner(q)],
                    seconds.at[k - 1, inner(q)],
                    rs_sent.at[2 + side],
                    rs_far.at[q, side],
                    peer,
                ).start()

    def return_stage(q):
        halves = []
        for side in range(2):
            seconds = (second_a, second_b)[side]
            settle(seconds.at[:, inner(q)], rs_far.at[q, side])
            own = sum_a[my, inner(q), :] if side == 0 else sum_b[mx, inner(q), :]
            summed = own.astype(jnp.float32)
            for k in range(spans[1 - side] - 1):
                summed = summed + seconds[k, inner(q), :].astype(jnp.float32)
            halves.append(summed)
        result = jnp.concatenate(halves, axis=0).astype(jnp.bfloat16)
        spread = fast_dot(spreading, result).astype(jnp.bfloat16)
        going_back[q * batch : (q + 1) * batch] = spread.reshape(batch, PAD, LANES)
        if q == 0:
            returned[me] = going_back[0]

        @pl.loop(q * batch if q else 1, (q + 1) * batch)
        def _(j):
            remote(
                going_back.at[j], returned.at[me], z_sent.at[1], z_recv.at[pieces], at_slot(j, 1)
            ).start()

    def active_copy(k):
        block = active.at[:, cols(mt)]
        return remote(block, block, act_sem.at[0], act_sem.at[1], in_plane(k))

    def carry_stage():
        turn = (grow[7][0], grow[7][1] * sign)
        lead = times(grow[6], grow[0])
        lead = (lead[0], lead[1] * sign)

        def absorb(j, pair):
            state, crossed = pair
            slot = carries.at[j]
            remote(slot, slot, carry_sem.at[0, 0], carry_sem.at[1, j], {"z": mz}).wait_recv()
            own, left = carries[j, 0:groups, :], carries[j, groups : 2 * groups, :]
            return (
                own + left * (turn[0] * state + turn[1] * crossed),
                pltpu.roll(own, LANES // 2, 1) + left * (turn[0] * crossed - turn[1] * state),
            )

        nothing = jnp.zeros((groups, LANES), jnp.float32)
        state, crossed = lax.fori_loop(0, me, absorb, (nothing, nothing))
        first = lead[0] * state + lead[1] * crossed
        first_crossed = lead[0] * crossed - lead[1] * state
        carried = jnp.zeros((length, LANES), jnp.float32)
        for g in range(groups):
            entering = powers[0, g] * first[g : g + 1, :] + powers[1, g] * first_crossed[g : g + 1, :]
            carried = carried + exact_dot(entering, of_group(read, g), ((1,), (1,)))
        active[:, cols(mt)] = jax.nn.gelu(partial[...] + fading[...] * carried).astype(jnp.bfloat16)

    for q in range(pieces):
        dispatch_stage(q)
        if q:
            forward_stage(q - 1)
    forward_stage(pieces - 1)
    carry_after = min(1, pieces - 1)
    for q in range(pieces + 2):
        if q < pieces:
            expert_stage(q)
        if q == carry_after:
            carry_stage()
        if 0 <= q - 1 < pieces:
            sum_stage(q - 1)
        if q == pieces:

            @pl.loop(1, tp)
            def _(k):
                active_copy(k).start()

        if 0 <= q - 2 < pieces:
            return_stage(q - 2)

    for load in loads[18:]:
        load.wait()
    settle(active.at[:, pl.ds(0, (tp - 1) * LANES)], act_sem.at[1])
    mixed = fast_dot(active[...], mix_w[...])
    mix_ref[...] = (mixed[:, :LANES] * jax.nn.sigmoid(mixed[:, LANES:])).astype(jnp.bfloat16)

    others = pl.ds(0, experts - 1)
    settle(returned.at[others], z_recv.at[pieces])
    every = returned[...].reshape(experts * PAD, LANES).astype(jnp.float32)
    moe_ref[...] = exact_dot(blend[...], every).astype(jnp.bfloat16)

    settle(outgoing.at[others], z_sent.at[0])
    settle(going_back.at[others], z_sent.at[1])
    settle(active.at[:, pl.ds(0, (tp - 1) * LANES)], act_sem.at[0])
    settle(gathered.at[:, pl.ds(0, (tp - 1) * LANES)], ag_sent.at[0])
    for at, ref in enumerate((first_a, first_b, second_a, second_b)):
        settle(ref, rs_sent.at[at])

    @pl.loop(1, experts)
    def _(k):
        @pl.when(me + k < experts)
        def _():
            carry_to(k).wait_send()


def local(
    sizes,
    mix_in,
    mix_gain,
    lam_re,
    lam_im,
    log_dt,
    b_re,
    b_im,
    c_re,
    c_im,
    d_skip,
    log_retain,
    w_lin,
    w_glu,
    moe_in,
    moe_gain,
    routes,
    route_weight,
    w_gate,
    w_up,
    w_down,
):
    nz, nc, ny, nx, capacity, pieces = sizes
    experts, tp = nz * nc, ny * nx
    groups, states, _ = b_re.shape
    flip = (0, 2, 1)
    args = (
        routes.T,
        route_weight.T,
        moe_in,
        moe_gain.reshape(1, -1),
        mix_in,
        mix_gain.reshape(1, -1),
        log_retain.T,
        lam_re,
        lam_im,
        log_dt.reshape(1, -1),
        b_re.transpose(flip).reshape(-1, states),
        b_im.transpose(flip).reshape(-1, states),
        c_re.reshape(-1, states),
        c_im.reshape(-1, states),
        d_skip.reshape(1, -1),
        w_gate[0],
        w_up[0],
        w_down[0],
        w_lin,
        w_glu,
    )
    length, tokens = mix_in.shape[0], moe_in.shape[0]
    slots, half, width = experts * capacity, experts * capacity // 2, tp * LANES
    f32, bf16 = jnp.float32, jnp.bfloat16
    dma = pltpu.SemaphoreType.DMA
    vmem = pl.BlockSpec(memory_space=pltpu.VMEM)
    return pl.pallas_call(
        functools.partial(exchange_kernel, sizes, len(args)),
        out_shape=(
            jax.ShapeDtypeStruct((length, LANES), bf16),
            jax.ShapeDtypeStruct((tokens, LANES), bf16),
        ),
        in_specs=[pl.BlockSpec(memory_space=pl.ANY)] * len(args),
        out_specs=(vmem, vmem),
        scratch_shapes=[
            *(pltpu.VMEM(a.shape, a.dtype) for a in args[:-2]),
            pltpu.VMEM((width, 2 * LANES), bf16),
            pltpu.VMEM((tokens, experts * PAD), f32),
            pltpu.VMEM((2, groups, length, LANES), f32),
            pltpu.VMEM((length, LANES), f32),
            pltpu.VMEM((length, LANES), f32),
            pltpu.VMEM((2 * groups, LANES), f32),
            pltpu.VMEM((experts, PAD, LANES), bf16),
            pltpu.VMEM((experts, PAD, LANES), bf16),
            pltpu.VMEM((experts, 2 * groups, LANES), f32),
            pltpu.VMEM((slots, width), bf16),
            pltpu.VMEM((ny, nx, slots, LANES), bf16),
            pltpu.VMEM((nx - 1, ny, half, LANES), bf16),
            pltpu.VMEM((ny - 1, nx, half, LANES), bf16),
            pltpu.VMEM((ny, half, LANES), bf16),
            pltpu.VMEM((nx, half, LANES), bf16),
            pltpu.VMEM((ny - 1, half, LANES), bf16),
            pltpu.VMEM((nx - 1, half, LANES), bf16),
            pltpu.VMEM((experts, PAD, LANES), bf16),
            pltpu.VMEM((experts, PAD, LANES), bf16),
            pltpu.VMEM((length, width), bf16),
            dma((len(args),)),
            dma((2,)),
            dma((pieces + 1,)),
            dma((2, experts)),
            dma((2,)),
            dma((pieces, 2, max(nx, ny))),
            dma((pieces, 2)),
            dma((1,)),
            dma((pieces, 2)),
            dma((pieces, 2)),
            dma((4,)),
        ],
        compiler_params=pltpu.CompilerParams(
            collective_id=0, has_side_effects=True, vmem_limit_bytes=56 * 1024 * 1024
        ),
    )(*args)


def solution(mesh, sizes=(16, 2, 4, 4, 12, 4)):
    torus = Mesh(mesh.devices.reshape(sizes[:4]), ("z", "c", "y", "x"))
    placed = (
        P(EP, None),
        P(),
        P(TP, None),
        P(TP, None),
        P(TP),
        P(TP, None, None),
        P(TP, None, None),
        P(TP, None, None),
        P(TP, None, None),
        P(TP),
        P(EP, TP),
        P(None, TP),
        P(None, TP),
        P(EP, None),
        P(),
        P(EP, None),
        P(EP, None),
        P(EP, None, TP),
        P(EP, None, TP),
        P(EP, TP, None),
    )
    return jax.shard_map(
        functools.partial(local, sizes),
        mesh=torus,
        in_specs=placed,
        out_specs=(P(EP, TP), P(EP, TP)),
        check_vma=False,
    )
```

profile of v0, /device:TPU:1, one launch (start us, length us, event | category | flops | bytes accessed | tf_op | source)
XLA Modules:
  0.0 71.5 jit_solution(10724463045681308984)
XLA Ops:
  0.6 68.8 %shard_map.203 = (bf16[128,128]{1,0:T(8,128)(2,1)}, bf16[128,128]{1,0:T(8,128)(2,1)}) custom-call(s32[2,128]{1,0:T(2,128)} %bitcast.28, f32[2,128]{1,0:T(2,128)} %bitcast.29, bf16[128,2048]{1,0:T(8,128)(2,1)} %refs_2_.1, f32[1,2048]{1,0:T(1,128)} %bitcast.25, bf16[128,2048]{1,0:T(8,128)(2,1)} %refs_4_.1, f32[1,2048]{1,0:T(1,128)} %bitcast.26, ...), custom_call_target="tpu_custom_call" | custom-call | tf_op jit(solution)/shard_map/pallas_call | solution.py:533
  69.5 0.0 copy-start
  69.5 1.4 %copy.24 = bf16[128,128]{1,0:T(8,128)(2,1)} copy(bf16[128,128]{1,0:T(8,128)(2,1)} %get-tuple-element.4) | data formatting | bytes 65536
  70.9 0.0 copy-done
  70.9 0.6 copy.25
Async XLA Ops:
  69.5 1.4 %copy-start = (bf16[128,128]{1,0:T(8,128)(2,1)S(1)}, bf16[128,128]{1,0:T(8,128)(2,1)}, u32[]{:S(2)}) copy-start(bf16[128,128]{1,0:T(8,128)(2,1)} %get-tuple-element.5) | copy-start | bytes 98308
where the time goes:
time: 71.7 us; the launch traced here: 71.5 us
  Pallas kernels  68.8 us (96%)
  local copies, waits for them, and re-layouts  2 us (3%)
    pallas_call x1, Pallas kernels, local(): pl.pallas_call(functools.partial(exchange_kernel, sizes, len(args)), out_...  68.8 us
    unnamed x4, local copies, waits for them, and re-layouts  2 us

commit v1 on v0

--- a/solution.py
+++ b/solution.py
@@ -15,6 +15,11 @@
 LANES = 128
 EPS = 1e-06
 HIGHEST = lax.Precision.HIGHEST
+ORDER = (
+    *("D0", "D1", "F0", "D2", "F1", "D3", "K", "F2", "F3"),
+    *("E1", "E2", "S1", "E3", "S2", "R1", "E0", "S3", "R2"),
+    *("C", "R3", "S0", "A", "R0"),
+)
 
 
 def cols(index):
@@ -44,7 +49,7 @@
 
 
 def exchange_kernel(sizes, count, *refs):
-    nz, nc, ny, nx, cap, pieces = sizes
+    nz, nc, ny, nx, cap, pieces, order = sizes
     experts, tp = nz * nc, ny * nx
     slots = experts * cap
     half = slots // 2
@@ -93,6 +98,10 @@
     def in_plane(k):
         peer = lax.rem(mt + k, tp)
         return {"y": lax.div(peer, nx), "x": lax.rem(peer, nx)}
+
+    filled = pl.ds(0, cap)
+    incoming[...] = jnp.zeros_like(incoming)
+    returned[...] = jnp.zeros_like(returned)
 
     barrier = pltpu.get_barrier_semaphore()
     reach = experts // 2
@@ -259,19 +268,20 @@
         @pl.loop(q * batch if q else 1, (q + 1) * batch)
         def _(j):
             peer = at_slot(j, -1)
-            block = outgoing.at[peer["z"] * nc + peer["c"]]
-            remote(block, incoming.at[j], z_sent.at[0], z_recv.at[q], peer).start()
+            block = outgoing.at[peer["z"] * nc + peer["c"], filled]
+            remote(block, incoming.at[j, filled], z_sent.at[0], z_recv.at[q], peer).start()
 
     def carry_to(k):
         return remote(
             message, carries.at[me], carry_sem.at[0, k], carry_sem.at[1, me], along_z(k)
         )
 
-    @pl.loop(1, experts)
-    def _(k):
-        @pl.when(me + k < experts)
-        def _():
-            carry_to(k).start()
+    def carry_sends():
+        @pl.loop(1, experts)
+        def _(k):
+            @pl.when(me + k < experts)
+            def _():
+                carry_to(k).start()
 
     def spot(side, q):
         return pl.ds(q * high + side * low, low)
@@ -305,7 +315,7 @@
 
     def dispatch_stage(q):
         low_slot = q * batch if q else 1
-        settle(incoming.at[pl.ds(low_slot, (q + 1) * batch - low_slot)], z_recv.at[q])
+        settle(incoming.at[pl.ds(low_slot, (q + 1) * batch - low_slot), filled], z_recv.at[q])
         blocks = incoming[q * batch : (q + 1) * batch].reshape(batch * PAD, LANES)
         packed = fast_dot(packing, blocks).astype(jnp.bfloat16)
         gathered[pl.ds(q * high, high), cols(mt)] = packed
@@ -330,9 +340,6 @@
         for side in range(2):
             distant = spans[side] * (spans[1 - side] - 1) * LANES
             settle(gathered.at[spot(side, q), pl.ds(0, distant)], ag_far.at[q, side])
-        if q == 0:
-            for load in loads[15:18]:
-                load.wait()
         features = gathered[q * high : (q + 1) * high, :]
         gate = fast_dot(features, gate_w[...])
         up = fast_dot(features, up_w[...])
@@ -397,7 +404,11 @@
         @pl.loop(q * batch if q else 1, (q + 1) * batch)
         def _(j):
             remote(
-                going_back.at[j], returned.at[me], z_sent.at[1], z_recv.at[pieces], at_slot(j, 1)
+                going_back.at[j, filled],
+                returned.at[me, filled],
+                z_sent.at[1],
+                z_recv.at[pieces],
+                at_slot(j, 1),
             ).start()
 
     def active_copy(k):
@@ -429,27 +440,25 @@
             carried = carried + exact_dot(entering, of_group(read, g), ((1,), (1,)))
         active[:, cols(mt)] = jax.nn.gelu(partial[...] + fading[...] * carried).astype(jnp.bfloat16)
 
-    for q in range(pieces):
-        dispatch_stage(q)
-        if q:
-            forward_stage(q - 1)
-    forward_stage(pieces - 1)
-    carry_after = min(1, pieces - 1)
-    for q in range(pieces + 2):
-        if q < pieces:
-            expert_stage(q)
-        if q == carry_after:
-            carry_stage()
-        if 0 <= q - 1 < pieces:
-            sum_stage(q - 1)
-        if q == pieces:
-
-            @pl.loop(1, tp)
-            def _(k):
-                active_copy(k).start()
-
-        if 0 <= q - 2 < pieces:
-            return_stage(q - 2)
+    def active_sends():
+        @pl.loop(1, tp)
+        def _(k):
+            active_copy(k).start()
+
+    stages = {
+        "D": dispatch_stage,
+        "F": forward_stage,
+        "E": expert_stage,
+        "S": sum_stage,
+        "R": return_stage,
+        "K": carry_sends,
+        "C": carry_stage,
+        "A": active_sends,
+    }
+    for load in loads[15:18]:
+        load.wait()
+    for step in order:
+        stages[step[0]](*(int(q) for q in step[1:]))
 
     for load in loads[18:]:
         load.wait()
@@ -458,12 +467,12 @@
     mix_ref[...] = (mixed[:, :LANES] * jax.nn.sigmoid(mixed[:, LANES:])).astype(jnp.bfloat16)
 
     others = pl.ds(0, experts - 1)
-    settle(returned.at[others], z_recv.at[pieces])
+    settle(returned.at[others, filled], z_recv.at[pieces])
     every = returned[...].reshape(experts * PAD, LANES).astype(jnp.float32)
     moe_ref[...] = exact_dot(blend[...], every).astype(jnp.bfloat16)
 
-    settle(outgoing.at[others], z_sent.at[0])
-    settle(going_back.at[others], z_sent.at[1])
+    settle(outgoing.at[others, filled], z_sent.at[0])
+    settle(going_back.at[others, filled], z_sent.at[1])
     settle(active.at[:, pl.ds(0, (tp - 1) * LANES)], act_sem.at[0])
     settle(gathered.at[:, pl.ds(0, (tp - 1) * LANES)], ag_sent.at[0])
     for at, ref in enumerate((first_a, first_b, second_a, second_b)):
@@ -499,7 +508,7 @@
     w_up,
     w_down,
 ):
-    nz, nc, ny, nx, capacity, pieces = sizes
+    nz, nc, ny, nx, capacity, pieces, _ = sizes
     experts, tp = nz * nc, ny * nx
     groups, states, _ = b_re.shape
     flip = (0, 2, 1)
@@ -578,7 +587,7 @@
     )(*args)
 
 
-def solution(mesh, sizes=(16, 2, 4, 4, 12, 4)):
+def solution(mesh, sizes=(16, 2, 4, 4, 12, 4, ORDER)):
     torus = Mesh(mesh.devices.reshape(sizes[:4]), ("z", "c", "y", "x"))
     placed = (
         P(EP, None),

time: 71.7 us -> 63.4 us (0.88)
  Pallas kernels: 68.8 us -> 60.6 us
    pallas_call x1, Pallas kernels: 68.8 us -> 60.6 us  [local(): pl.pallas_call(functools.partial(exchange_kernel, sizes, len(args)), out_...]
where the time goes in v1:
time: 63.4 us; the launch traced here: 63.2 us
  Pallas kernels  60.6 us (96%)
  local copies, waits for them, and re-layouts  2 us (3%)
  between operations  0.66 us (1%)
    pallas_call x1, Pallas kernels, local(): pl.pallas_call(functools.partial(exchange_kernel, sizes, len(args)), out_...  60.6 us
    unnamed x4, local copies, waits for them, and re-layouts  2 us

profile of v1, /device:TPU:1, one launch (start us, length us, event | category | flops | bytes accessed | tf_op | source)
XLA Modules:
  0.0 63.2 jit_solution(2455934640549800266)
XLA Ops:
  0.6 60.6 %shard_map.203 = (bf16[128,128]{1,0:T(8,128)(2,1)}, bf16[128,128]{1,0:T(8,128)(2,1)}) custom-call(s32[2,128]{1,0:T(2,128)} %bitcast.28, f32[2,128]{1,0:T(2,128)} %bitcast.29, bf16[128,2048]{1,0:T(8,128)(2,1)} %refs_2_.1, f32[1,2048]{1,0:T(1,128)} %bitcast.25, bf16[128,2048]{1,0:T(8,128)(2,1)} %refs_4_.1, f32[1,2048]{1,0:T(1,128)} %bitcast.26, ...), custom_call_target="tpu_custom_call" | custom-call | tf_op jit(solution)/shard_map/pallas_call | solution.py:542
  61.2 0.0 copy-start
  61.2 1.4 %copy.24 = bf16[128,128]{1,0:T(8,128)(2,1)} copy(bf16[128,128]{1,0:T(8,128)(2,1)} %get-tuple-element.4) | data formatting | bytes 65536
  62.6 0.0 copy-done
  62.6 0.6 copy.25
Async XLA Ops:
  61.2 1.4 %copy-start = (bf16[128,128]{1,0:T(8,128)(2,1)S(1)}, bf16[128,128]{1,0:T(8,128)(2,1)}, u32[]{:S(2)}) copy-start(bf16[128,128]{1,0:T(8,128)(2,1)} %get-tuple-element.5) | copy-start | bytes 98308

commit v2 on v1

--- a/solution.py
+++ b/solution.py
@@ -16,7 +16,7 @@
 EPS = 1e-06
 HIGHEST = lax.Precision.HIGHEST
 ORDER = (
-    *("D0", "D1", "F0", "D2", "F1", "D3", "K", "F2", "F3"),
+    *("D0", "D1", "F0", "D2", "K", "F1", "D3", "F2", "F3"),
     *("E1", "E2", "S1", "E3", "S2", "R1", "E0", "S3", "R2"),
     *("C", "R3", "S0", "A", "R0"),
 )
@@ -56,7 +56,7 @@
     batch = experts // pieces
     high, low = batch * cap, batch * cap // 2
     sources, refs = refs[:count], refs[count:]
-    (mix_ref, moe_ref), refs = refs[:2], refs[2:]
+    (out_ref,), refs = refs[:1], refs[1:]
     staged, refs = refs[: count - 2], refs[count - 2 :]
     (mix_w, blend, powers, partial, fading, message, outgoing, incoming, carries), refs = (
         refs[:9],
@@ -303,6 +303,8 @@
         return {"y": lax.rem(my + k, ny)}
 
     spans = (nx, ny)
+    widest = max(nx, ny)
+    nearest_first = sorted(range(1, widest), key=lambda k: min(k, widest - k))
 
     def near_copy(side, q, k):
         block = gathered.at[spot(side, q), cols(mt)]
@@ -326,7 +328,7 @@
             forward(side, q, mt)
 
     def forward_stage(q):
-        for k in range(1, max(nx, ny)):
+        for k in nearest_first:
             for side in range(2):
                 if k < spans[side]:
                     near_copy(side, q, k).wait_recv()
@@ -464,12 +466,12 @@
         load.wait()
     settle(active.at[:, pl.ds(0, (tp - 1) * LANES)], act_sem.at[1])
     mixed = fast_dot(active[...], mix_w[...])
-    mix_ref[...] = (mixed[:, :LANES] * jax.nn.sigmoid(mixed[:, LANES:])).astype(jnp.bfloat16)
+    out_ref[0] = (mixed[:, :LANES] * jax.nn.sigmoid(mixed[:, LANES:])).astype(jnp.bfloat16)
 
     others = pl.ds(0, experts - 1)
     settle(returned.at[others, filled], z_recv.at[pieces])
     every = returned[...].reshape(experts * PAD, LANES).astype(jnp.float32)
-    moe_ref[...] = exact_dot(blend[...], every).astype(jnp.bfloat16)
+    out_ref[1] = exact_dot(blend[...], every).astype(jnp.bfloat16)
 
     settle(outgoing.at[others, filled], z_sent.at[0])
     settle(going_back.at[others, filled], z_sent.at[1])
@@ -539,14 +541,11 @@
     f32, bf16 = jnp.float32, jnp.bfloat16
     dma = pltpu.SemaphoreType.DMA
     vmem = pl.BlockSpec(memory_space=pltpu.VMEM)
-    return pl.pallas_call(
+    both = pl.pallas_call(
         functools.partial(exchange_kernel, sizes, len(args)),
-        out_shape=(
-            jax.ShapeDtypeStruct((length, LANES), bf16),
-            jax.ShapeDtypeStruct((tokens, LANES), bf16),
-        ),
+        out_shape=jax.ShapeDtypeStruct((2, length, LANES), bf16),
         in_specs=[pl.BlockSpec(memory_space=pl.ANY)] * len(args),
-        out_specs=(vmem, vmem),
+        out_specs=vmem,
         scratch_shapes=[
             *(pltpu.VMEM(a.shape, a.dtype) for a in args[:-2]),
             pltpu.VMEM((width, 2 * LANES), bf16),
@@ -585,6 +584,7 @@
             collective_id=0, has_side_effects=True, vmem_limit_bytes=56 * 1024 * 1024
         ),
     )(*args)
+    return both[0], both[1]
 
 
 def solution(mesh, sizes=(16, 2, 4, 4, 12, 4, ORDER)):

time: 63.4 us -> 62.5 us (0.986)
    unnamed x4 -> x0, local copies, waits for them, and re-layouts: 2 us -> none
    squeeze x0 -> x1, local copies, waits for them, and re-layouts: none -> 1.4 us  [local(): return (both[0], both[1])]
where the time goes in v2:
time: 62.5 us; the launch traced here: 62.3 us
  Pallas kernels  60.2 us (96%)
  local copies, waits for them, and re-layouts  1.4 us (2%)
  between operations  0.65 us (1%)
    pallas_call x1, Pallas kernels, local(): pl.pallas_call(functools.partial(exchange_kernel, sizes, len(args)), out_...  60.2 us
    squeeze x1, local copies, waits for them, and re-layouts, local(): return (both[0], both[1])  1.4 us

profile of v2, /device:TPU:1, one launch (start us, length us, event | category | flops | bytes accessed | tf_op | source)
XLA Modules:
  0.0 62.3 jit_solution(10398662648528407002)
XLA Ops:
  0.6 60.2 %shard_map.203 = bf16[2,128,128]{2,1,0:T(8,128)(2,1)} custom-call(s32[2,128]{1,0:T(2,128)} %bitcast.32, f32[2,128]{1,0:T(2,128)} %bitcast.33, bf16[128,2048]{1,0:T(8,128)(2,1)} %refs_2_.1, f32[1,2048]{1,0:T(1,128)} %bitcast.29, bf16[128,2048]{1,0:T(8,128)(2,1)} %refs_4_.1, f32[1,2048]{1,0:T(1,128)} %bitcast.30, f32[8,128]{1,0:T(8,128)} %bitcast.31, ...), custom_call_target="tpu_custom_call" | custom-call | tf_op jit(solution)/shard_map/pallas_call | solution.py:544
  60.9 1.4 %slice_bitcast_fusion = (bf16[128,128]{1,0:T(8,128)(2,1)}, bf16[128,128]{1,0:T(8,128)(2,1)}) fusion(bf16[2,128,128]{2,1,0:T(8,128)(2,1)} %shard_map.203), kind=kLoop, calls=%fused_computation | loop fusion | bytes 131072 | tf_op jit(solution)/shard_map/squeeze | solution.py:587
